TPU v7x, 32 devices: a whole 2x2x4 slice. The times are simulated.
32 devices in a mesh: rep: 2 (over y), fs: 4 (over z), tp: 4 (over x, core).
Axes of the slice: x: 2, y: 2, z: 4, core: 2. Of those that a mesh axis runs over, the one named last changes fastest.
Arguments:
- tokens: bfloat16 [2048, 2048], P(('rep', 'fs')), may hold values from -6 to 6
- mix_gain: float32 [2048], replicated, may hold values from 0.1 to 1.9
- group_weight: float32 [512, 2048], P('fs', 'tp'), may hold values from -0.25 to 0.25
- group_scale: float32 [1, 2048], P(None, 'tp'), may hold values from 0.5 to 2
- mlp_gain: float32 [2048], replicated, may hold values from 0.1 to 1.9
- up_weight: float32 [2048, 8192], P('fs', 'tp'), may hold values from -0.125 to 0.125
- up_scale: float32 [1, 8192], P(None, 'tp'), may hold values from 0.5 to 2
- down_weight: float32 [8192, 2048], P('tp', 'fs'), may hold values from -0.0625 to 0.0625
- down_scale: float32 [1, 2048], replicated, may hold values from 0.5 to 2
Outputs:
- layer_out: bfloat16 [2048, 2048], P(('rep', 'fs'))
All inputs are finite; a program needn't handle non-finite values.
Results may differ from a plain program's by a relative error of at most 0.013.
Values may be sent and summed in bfloat16 or wider, within the bound.
A program may use at most 64 MiB of HBM per device.

v0:
```python
import jax
import jax.numpy as jnp
from jax import lax
from jax.sharding import PartitionSpec as P

GROUPS = 4
LENGTH = 128


norm_eps = 1e-06


def norm_rows(values, gain):
    promoted = values.astype(jnp.float32)
    inverse = lax.rsqrt(jnp.mean(promoted * promoted, axis=-1, keepdims=True) + norm_eps)
    return (promoted * inverse * gain).astype(jnp.bfloat16)


def band_means(inputs, window, seq_length):
    row_count, columns = inputs.shape
    by_sequence = inputs.reshape(row_count // seq_length, seq_length, columns)
    position = jnp.arange(seq_length, dtype=jnp.int32)
    offset = position[:, None] - position[None, :]
    band_mask = ((offset >= 0) & (offset < window)).astype(jnp.bfloat16)
    divisor = jnp.minimum(position + 1, window).astype(jnp.float32)
    summed = jnp.einsum("ts,nsc->ntc", band_mask, by_sequence, preferred_element_type=jnp.float32)
    return (summed / divisor[None, :, None] - by_sequence.astype(jnp.float32)).reshape(
        row_count, columns
    )


def body(
    tokens,
    mix_gain,
    group_weight,
    group_scale,
    mlp_gain,
    up_weight,
    up_scale,
    down_weight,
    down_scale,
):
    model_width = tokens.shape[1]
    group_width = model_width // GROUPS
    own_cols = group_weight.shape[1]
    column_start = lax.axis_index("tp") * own_cols
    group_index = column_start // group_width
    normed = norm_rows(tokens, mix_gain)
    inputs = lax.dynamic_slice_in_dim(normed, group_index * group_width, group_width, 1)
    window = jnp.left_shift(jnp.int32(2), group_index)
    pooled = band_means(inputs, window, LENGTH).astype(jnp.bfloat16)
    mixed_cols = (
        jnp.dot(
            pooled,
            lax.all_gather(group_weight.astype(jnp.bfloat16), "fs", axis=0, tiled=True),
            preferred_element_type=jnp.float32,
        )
        * group_scale
    )
    own_tokens = lax.dynamic_slice_in_dim(tokens, column_start, own_cols, 1)
    carried_cols = (own_tokens.astype(jnp.float32) + mixed_cols).astype(jnp.bfloat16)
    carried = lax.all_gather(carried_cols, "tp", axis=1, tiled=True)
    normed_mlp = norm_rows(carried, mlp_gain)
    pre_act = (
        jnp.dot(
            normed_mlp,
            lax.all_gather(up_weight.astype(jnp.bfloat16), "fs", axis=0, tiled=True),
            preferred_element_type=jnp.float32,
        )
        * up_scale
    )
    hidden = jnp.square(jax.nn.relu(pre_act)).astype(jnp.bfloat16)
    partial_value = (
        jnp.dot(
            hidden,
            lax.all_gather(down_weight.astype(jnp.bfloat16), "fs", axis=1, tiled=True),
            preferred_element_type=jnp.float32,
        )
        * down_scale
    )
    summed = lax.psum(partial_value.astype(jnp.bfloat16), "tp").astype(jnp.float32)
    return (carried.astype(jnp.float32) + summed).astype(jnp.bfloat16)


def solution(mesh):
    in_specs = (
        P(("rep", "fs"), None),
        P(),
        P("fs", "tp"),
        P(None, "tp"),
        P(),
        P("fs", "tp"),
        P(None, "tp"),
        P("tp", "fs"),
        P(),
    )
    out_specs = P(("rep", "fs"), None)
    return jax.shard_map(body, mesh=mesh, in_specs=in_specs, out_specs=out_specs, check_vma=False)
```

profile of v0, /device:TPU:1, one launch (start us, length us, event | category | flops | bytes accessed | tf_op | source)
XLA Modules:
  0.0 403.8 jit_solution(14775882686962388429)
XLA Ops:
  6.5 0.0 all-gather.4.cloned.1.call-start
  6.5 0.0 copy-start.1
  6.5 1.6 multiply_reduce_fusion
  8.1 1.5 convert_element_type.58
  9.6 0.0 copy-start.2
  9.6 0.0 copy-done.1
  9.6 15.3 %all_gather.12 = bf16[512,512]{1,0:T(8,128)(2,1)S(1)} all-gather(bf16[128,512]{1,0:T(8,128)(2,1)S(1)} %convert_element_type.64), channel_id=1, replica_groups=mesh['rep'=2,'fs'=4,'tp'=4] {'fs'}, dimensions={0}, use_global_device_ids=true | all-gather | bytes 655360 | tf_op jit(solution)/shard_map/all_gather | solution.py:55
  25.0 0.8 dynamic-slice
  25.7 0.1 fusion.19
  25.8 0.2 fusion.12
  26.1 0.0 copy-done.2
  26.1 2.0 fusion.11
  28.0 0.0 all-gather.4.cloned.1.call-update
  28.1 0.0 all-gather.6.cloned.1.call-start
  28.1 3.8 convert_element_type.68
  32.0 0.0 all-gather.6.cloned.1.call-update
  32.0 0.0 all-gather.8.cloned.1.call-start
  32.0 3.8 convert_element_type.70
  35.8 0.0 all-gather.8.cloned.1.call-update
  35.8 0.0 all-reduce.2.cloned.1.call-start
  35.9 12.6 %all-gather.4.cloned.1.call-done = bf16[256,2048]{1,0:T(8,128)(2,1)} async-done(((bf16[256,512]{1,0:T(8,128)(2,1)}), bf16[256,2048]{1,0:T(8,128)(2,1)}) %all-gather.4.cloned.1.call-update) | async-done | bytes 1048592 | tf_op jit(solution)/shard_map/all_gather | solution.py:62
  48.5 1.5 fusion.4
  50.0 149.5 %all-gather.6.cloned.1.call-done = bf16[2048,2048]{1,0:T(8,128)(2,1)} async-done(((bf16[512,2048]{1,0:T(8,128)(2,1)}), bf16[2048,2048]{1,0:T(8,128)(2,1)}) %all-gather.6.cloned.1.call-update) | async-done | bytes 8388624 | tf_op jit(solution)/shard_map/all_gather | solution.py:67
  199.4 149.4 %all-gather.8.cloned.1.call-done = bf16[2048,2048]{1,0:T(8,128)(2,1)} async-done(((bf16[2048,512]{1,0:T(8,128)(2,1)}), bf16[2048,2048]{1,0:T(8,128)(2,1)}) %all-gather.8.cloned.1.call-update) | async-done | bytes 8388624 | tf_op jit(solution)/shard_map/all_gather | solution.py:76
  348.9 0.0 copy-done.3
  348.9 0.0 copy-done.4
  348.9 0.0 copy-done.5
  348.9 11.7 %fusion.2 = bf16[256,2048]{1,0:T(8,128)(2,1)} fusion(bf16[2048,2048]{1,0:T(8,128)(2,1)} %all-gather.8.cloned.1.call-done, f32[2048]{0:T(1024)S(1)} %bitcast.22, bf16[2048,2048]{1,0:T(8,128)(2,1)} %all-gather.6.cloned.1.call-done, bf16[256,2048]{1,0:T(8,128)(2,1)} %all-gather.4.cloned.1.call-done, f32[2048]{0:T(1024)S(1)} %bitcast.23, ...), kind=kOutput, calls=%fused_computation.7 | convolution fusion | flops 4300210176 | bytes 18899968 | tf_op jit(solution)/shard_map/dot_general | solution.py:74
  360.6 0.0 all-reduce.2.cloned.1.call-update
  360.6 34.1 %all-reduce.2.cloned.1.call-done = bf16[256,2048]{1,0:T(8,128)(2,1)} async-done(((bf16[256,2048]{1,0:T(8,128)(2,1)}), bf16[256,2048]{1,0:T(8,128)(2,1)}) %all-reduce.2.cloned.1.call-update) | async-done | bytes 1048592 | tf_op jit(solution)/shard_map/psum | solution.py:81
  394.7 0.0 copy-done
  394.7 2.6 fusion.7
  (8 shorter events, 0.0 us)
Async XLA Ops:
  6.5 41.9 %all-gather.4.cloned.1.call-start = ((), (), s32[]{:S(2)}) async-start(), calls=%async_computation | async-start | bytes 1310720 | tf_op jit(solution)/shard_map/all_gather | solution.py:62
  6.5 3.1 copy-start.1
  9.6 16.5 %copy-start.2 = (f32[1,512]{1,0:T(1,128)S(1)}, f32[1,512]{1,0:T(1,128)}, u32[]{:S(2)}) copy-start(f32[1,512]{1,0:T(1,128)} %param.12) | copy-start | bytes 6148
  28.1 171.4 %all-gather.6.cloned.1.call-start = ((), (), s32[]{:S(2)}) async-start(), calls=%async_computation.1 | async-start | bytes 10485760 | tf_op jit(solution)/shard_map/all_gather | solution.py:67
  32.0 316.9 %all-gather.8.cloned.1.call-start = ((), (), s32[]{:S(2)}) async-start(), calls=%async_computation.2 | async-start | bytes 10485760 | tf_op jit(solution)/shard_map/all_gather | solution.py:76
  35.8 313.1 %copy-start.3 = (f32[1,2048]{1,0:T(1,128)S(1)}, f32[1,2048]{1,0:T(1,128)}, u32[]{:S(2)}) copy-start(f32[1,2048]{1,0:T(1,128)} %param.17) | copy-start | bytes 24580
  35.8 313.1 %copy-start.4 = (f32[1,2048]{1,0:T(1,128)S(1)}, f32[1,2048]{1,0:T(1,128)}, u32[]{:S(2)}) copy-start(f32[1,2048]{1,0:T(1,128)} %param.15) | copy-start | bytes 24580
  35.8 313.1 %copy-start.5 = (f32[2048]{0:T(1024)S(1)}, f32[2048]{0:T(1024)}, u32[]{:S(2)}) copy-start(f32[2048]{0:T(1024)} %param.13) | copy-start | bytes 24580
  35.8 358.9 %all-reduce.2.cloned.1.call-start = ((), (), s32[]{:S(2)}) async-start(), calls=%async_computation.3 | async-start | bytes 2097152 | tf_op jit(solution)/shard_map/psum | solution.py:81
  348.9 45.8 %copy-start = (bf16[256,2048]{1,0:T(8,128)(2,1)S(1)}, bf16[256,2048]{1,0:T(8,128)(2,1)}, u32[]{:S(2)}) copy-start(bf16[256,2048]{1,0:T(8,128)(2,1)} %all-gather.4.cloned.1.call-done) | copy-start | bytes 3145732
Sparse Core Ops, SparseCore 0:
  28.2 20.2 all-gather.3
  50.0 149.3 all-gather.5
  201.0 147.7 all-gather.7
  360.7 33.9 all-reduce.1
where the time goes:
time: 405 us; the launch traced here: 404 us
  waiting for transfers between devices  346 us (85%)
  blocking collectives  15.3 us (4%)
  other arithmetic  14.9 us (4%)
  matrix products  13.9 us (3%)
  between operations  13.2 us (3%)
    all_gather x1, waiting for transfers between devices, body(): lax.all_gather(up_weight.astype(jnp.bfloat16), 'fs', axis=0, tiled=True)  149 us
    all_gather x1, waiting for transfers between devices, body(): lax.all_gather(down_weight.astype(jnp.bfloat16), 'fs', axis=1, tiled=True)  149 us
    psum x1, waiting for transfers between devices, body(): lax.psum(partial_value.astype(jnp.bfloat16), 'tp').astype(jnp.float32)  34.1 us
    all_gather x1, blocking collectives, body(): lax.all_gather(group_weight.astype(jnp.bfloat16), 'fs', axis=0, tiled=True)  15.3 us
    all_gather x1, waiting for transfers between devices, body(): carried = lax.all_gather(carried_cols, 'tp', axis=1, tiled=True)  12.6 us
    dot_general x1, matrix products, body(): jnp.dot(hidden, lax.all_gather(down_weight.astype(jnp.bfloat16), 'fs', ax...  11.7 us
  transfers between devices with their start and end apart: 4, of which 4 were waited for; matrix products, arithmetic and copies ran while one was open for 2% of the time, Pallas kernels for 0%

commit v1 on v0

--- a/solution.py
+++ b/solution.py
@@ -1,6 +1,10 @@
+import functools
+
 import jax
 import jax.numpy as jnp
 from jax import lax
+from jax.experimental import pallas as pl
+from jax.experimental.pallas import tpu as pltpu
 from jax.sharding import PartitionSpec as P
 
 GROUPS = 4
@@ -82,6 +86,289 @@
     return (carried.astype(jnp.float32) + summed).astype(jnp.bfloat16)
 
 
+MESH = pl.DeviceIdType.MESH
+
+
+def ring_kernel(
+    sizes,
+    tok_h, mg, gw_h, gs, lg, up_h, us, dn_h, ds,
+    out_h,
+    tok, gwf, upf, upo, dnf, dno,
+    gwg, ups, upg, dns, dng,
+    car, xn, pb, ra, sx, rb, sz, rc, og,
+    ld, sw, rw, sy, ry, scz, rcz, scx, rcx, scc, rcc,
+    sa, ra_s, sb, rb_s, st, rt, so, ro, wr,
+):
+    Z, T, rows, D, own, hg, hu, hd, fsub, dsub = sizes
+    r, z, t = lax.axis_index("rep"), lax.axis_index("fs"), lax.axis_index("tp")
+    cp = t + 1 - 2 * lax.rem(t, 2)
+    xp = lax.rem(t + 2, T)
+    cxp = lax.rem(cp + 2, T)
+    peer_r = 1 - r
+    bf, f32 = jnp.bfloat16, jnp.float32
+
+    def mul(i, n):
+        return pl.multiple_of(i * n, n)
+
+    def zat(d):
+        return lax.rem(z + d, Z)
+
+    loads = {}
+
+    def load(key, src, dst, k):
+        c = pltpu.make_async_copy(src, dst, ld.at[k])
+        c.start()
+        loads[key] = c
+
+    load("gw", gw_h, gwf, 0)
+    load("tok", tok_h, tok, 1)
+    order = list(range(1, Z)) + [0]
+    for i, d in enumerate(order):
+        zd = zat(d)
+        load(("up", d), up_h.at[pl.ds(mul(r, hu), hu), pl.ds(mul(zd, fsub), fsub)], upf.at[d], 2 + d)
+        load(("dn", d), dn_h.at[pl.ds(pl.multiple_of(zd * 2 * hd + r * hd, hd), hd), :], dnf.at[d], 2 + Z + d)
+    load("upo", up_h.at[pl.ds(mul(peer_r, hu), hu), pl.ds(mul(z, fsub), fsub)], upo, 2 + 2 * Z)
+    load("dno", dn_h.at[pl.ds(pl.multiple_of(z * 2 * hd + peer_r * hd, hd), hd), :], dno, 3 + 2 * Z)
+
+    barrier = pltpu.get_barrier_semaphore()
+    peers = [(r, zat(d), t) for d in range(1, Z)] + [(peer_r, z, t), (r, z, xp), (r, z, cp)]
+    for p in peers:
+        pl.semaphore_signal(barrier, inc=1, device_id=p, device_id_type=MESH)
+    pl.semaphore_wait(barrier, len(peers))
+
+    sends = []
+
+    def remote(src, dst, ss, rs, dev):
+        return pltpu.make_async_remote_copy(
+            src_ref=src, dst_ref=dst, send_sem=ss, recv_sem=rs, device_id=dev, device_id_type=MESH
+        )
+
+    def send(src, dst, ss, rs, dev):
+        c = remote(src, dst, ss, rs, dev)
+        c.start()
+        sends.append(c)
+
+    def got(dst, ss, rs):
+        remote(dst, dst, ss, rs, (peer_r, z, t)).wait_recv()
+
+    def gw_at(src, rep):
+        return gwg.at[pl.ds(pl.multiple_of(src * 2 * hg + rep * hg, hg), hg), :]
+
+    def up_at(src, rep):
+        return upg.at[pl.ds(pl.multiple_of(src * 2 * hu + rep * hu, hu), hu), :]
+
+    def dn_at(src, rep):
+        return dng.at[src, pl.ds(mul(rep, hd), hd), :]
+
+    place = (gw_at, up_at, dn_at)
+
+    loads["gw"].wait()
+    gwg[pl.ds(mul(z, 2 * hg), 2 * hg), :] = gwf[...].astype(bf)
+    for i, d in enumerate(range(1, Z)):
+        loads[("up", d)].wait()
+        ups[d] = upf[d].astype(bf)
+        if i == 0:
+            for e in range(1, Z):
+                send(gw_at(z, r), gw_at(z, r), sw.at[0, e], rw.at[0, z], (r, zat(e), t))
+        loads[("dn", d)].wait()
+        dns[d] = dnf[d].astype(bf)
+    for d in range(1, Z):
+        send(ups.at[d], up_at(z, r), sw.at[1, d], rw.at[1, z], (r, zat(d), t))
+    for d in range(1, Z):
+        send(dns.at[d], dn_at(z, r), sw.at[2, d], rw.at[2, z], (r, zat(d), t))
+    loads[("up", 0)].wait()
+    upg[pl.ds(pl.multiple_of(z * 2 * hu + r * hu, hu), hu), :] = upf[0].astype(bf)
+    loads["upo"].wait()
+    upg[pl.ds(pl.multiple_of(z * 2 * hu + peer_r * hu, hu), hu), :] = upo[...].astype(bf)
+    loads[("dn", 0)].wait()
+    dng[z, pl.ds(mul(r, hd), hd), :] = dnf[0].astype(bf)
+    loads["dno"].wait()
+    dng[z, pl.ds(mul(peer_r, hd), hd), :] = dno[...].astype(bf)
+
+    loads["tok"].wait()
+    full = tok[...].astype(f32)
+    inv = lax.rsqrt(jnp.mean(full * full, axis=-1, keepdims=True) + norm_eps)
+    cols = pl.ds(mul(t, own), own)
+    mine = tok[:, cols].astype(f32)
+    normed = (mine * inv * mg[:, cols]).astype(bf)
+    window = jnp.left_shift(jnp.int32(2), t)
+    ti = lax.broadcasted_iota(jnp.int32, (LENGTH, LENGTH), 0)
+    si = lax.broadcasted_iota(jnp.int32, (LENGTH, LENGTH), 1)
+    band = jnp.where((ti - si >= 0) & (ti - si < window), 1.0, 0.0).astype(bf)
+    pos = lax.broadcasted_iota(jnp.int32, (LENGTH, own), 0)
+    divisor = jnp.minimum(pos + 1, window).astype(f32)
+    pooled = []
+    for s in range(rows // LENGTH):
+        part = normed[s * LENGTH:(s + 1) * LENGTH]
+        summed = jnp.dot(band, part, preferred_element_type=f32)
+        pooled.append((summed / divisor - part.astype(f32)).astype(bf))
+    pooled = jnp.concatenate(pooled, axis=0)
+
+    def swap(w):
+        for d in range(1, Z):
+            src = zat(Z - d)
+            got(place[w](src, r), sw.at[w, d], rw.at[w, src])
+            send(place[w](src, r), place[w](src, r), sy.at[w, d], ry.at[w, src], (peer_r, z, t))
+
+    def swapped(w):
+        for d in range(1, Z):
+            src = zat(Z - d)
+            got(place[w](src, peer_r), sy.at[w, d], ry.at[w, src])
+
+    swap(0)
+    swapped(0)
+    mixed = jnp.dot(pooled, gwg[...], preferred_element_type=f32) * gs[...]
+    car[z, t] = (mine + mixed).astype(bf)
+    blk = car.at[z, t]
+    send(blk, blk, scx.at[0], rcx.at[z], (r, z, xp))
+    send(blk, blk, scc.at[0, 0], rcc.at[z, 0], (r, z, cp))
+    for d in range(1, Z):
+        send(blk, blk, scz.at[d], rcz.at[z], (r, zat(d), t))
+
+    def from_x(d):
+        src = zat(Z - d)
+        got(car.at[src, xp], scx.at[d], rcx.at[src])
+        b = car.at[src, xp]
+        send(b, b, scc.at[d, 1], rcc.at[src, 1], (r, z, cp))
+
+    swap(1)
+    from_x(0)
+    swap(2)
+    for d in range(1, Z):
+        src = zat(Z - d)
+        b = car.at[src, t]
+        got(b, scz.at[d], rcz.at[src])
+        send(b, b, scx.at[d], rcx.at[src], (r, z, xp))
+        send(b, b, scc.at[d, 0], rcc.at[src, 0], (r, z, cp))
+    swapped(1)
+    swapped(2)
+
+    def compute(d):
+        src = zat(Z - d)
+        if d > 0:
+            from_x(d)
+        got(car.at[src, cp], scc.at[d, 0], rcc.at[src, 0])
+        got(car.at[src, cxp], scc.at[d, 1], rcc.at[src, 1])
+        total = jnp.zeros((rows, 1), f32)
+        for q in range(T):
+            c = car[src, q].astype(f32)
+            total += jnp.sum(c * c, axis=-1, keepdims=True)
+        scale = lax.rsqrt(total / D + norm_eps)
+        for q in range(T):
+            part = slice(q * own, (q + 1) * own)
+            xn[:, part] = (car[src, q].astype(f32) * scale * lg[:, part]).astype(bf)
+        pre = jnp.dot(xn[...], upg[...], preferred_element_type=f32)
+        pre = jnp.maximum(pre * us[:, pl.ds(mul(z, fsub), fsub)], 0.0)
+        hidden = (pre * pre).astype(bf)
+        for q in range(T):
+            part = slice(q * own, (q + 1) * own)
+            p = jnp.dot(hidden, dng[q], preferred_element_type=f32) * ds[:, part]
+            pb[src, q] = p.astype(bf)
+        send(pb.at[src, cxp], ra.at[src, 1], sa.at[d, 1], ra_s.at[src, 1], (r, z, cp))
+        send(pb.at[src, cp], ra.at[src, 0], sa.at[d, 0], ra_s.at[src, 0], (r, z, cp))
+
+    def over_x(d):
+        src = zat(Z - d)
+        got(ra.at[src, 1], sa.at[d, 1], ra_s.at[src, 1])
+        sx[src] = (pb[src, xp].astype(f32) + ra[src, 1].astype(f32)).astype(bf)
+        send(sx.at[src], rb.at[src], sb.at[d], rb_s.at[src], (r, z, xp))
+
+    def over_z(d):
+        src = zat(Z - d)
+        got(ra.at[src, 0], sa.at[d, 0], ra_s.at[src, 0])
+        got(rb.at[src], sb.at[d], rb_s.at[src])
+        both = pb[src, t].astype(f32) + ra[src, 0].astype(f32) + rb[src].astype(f32)
+        if d == 0:
+            return both
+        sz[src] = both.astype(bf)
+        send(sz.at[src], rc.at[z], st.at[d], rt.at[z], (r, src, t))
+
+    kept = None
+    for i in range(Z + 2):
+        if i < Z:
+            compute(i)
+        if 0 <= i - 1 < Z:
+            over_x(i - 1)
+        if 0 <= i - 2 < Z:
+            if i - 2 > 0:
+                over_z(i - 2)
+    acc = over_z(0)
+    acc += car[z, t].astype(f32)
+    for d in range(1, Z):
+        src = zat(d)
+        got(rc.at[src], st.at[d], rt.at[src])
+        acc += rc[src].astype(f32)
+    og[t] = acc.astype(bf)
+    send(og.at[t], og.at[t], so.at[0], ro.at[0], (r, z, xp))
+    send(og.at[t], og.at[t], so.at[1], ro.at[1], (r, z, cp))
+    writes = []
+
+    def write(q, k):
+        c = pltpu.make_async_copy(og.at[q], out_h.at[:, pl.ds(mul(q, own), own)], wr.at[k])
+        c.start()
+        writes.append(c)
+
+    write(t, 0)
+    got(og.at[xp], so.at[0], ro.at[0])
+    send(og.at[xp], og.at[xp], so.at[2], ro.at[2], (r, z, cp))
+    write(xp, 1)
+    got(og.at[cp], so.at[1], ro.at[1])
+    write(cp, 2)
+    got(og.at[cxp], so.at[2], ro.at[2])
+    write(cxp, 3)
+    for c in sends:
+        c.wait_send()
+    for c in writes:
+        c.wait()
+
+
+def fused(mesh_shape, tokens, mix_gain, group_weight, group_scale, mlp_gain, up_weight, up_scale, down_weight, down_scale):
+    Z, T = mesh_shape["fs"], mesh_shape["tp"]
+    rows, D = tokens.shape
+    own = group_weight.shape[1]
+    hg, hu = group_weight.shape[0] // 2, up_weight.shape[0] // 2
+    fsub = up_weight.shape[1] // Z
+    hd = fsub // 2
+    dsub = down_weight.shape[1]
+    bf, f32 = jnp.bfloat16, jnp.float32
+    dma = pltpu.SemaphoreType.DMA
+    vm = pl.BlockSpec(memory_space=pltpu.VMEM)
+    hbm = pl.BlockSpec(memory_space=pl.ANY)
+    sizes = (Z, T, rows, D, own, hg, hu, hd, fsub, dsub)
+    V = pltpu.VMEM
+    block = (Z, rows, own)
+    return pl.pallas_call(
+        functools.partial(ring_kernel, sizes),
+        out_shape=jax.ShapeDtypeStruct((rows, D), bf),
+        in_specs=[hbm, vm, hbm, vm, vm, hbm, vm, hbm, vm],
+        out_specs=hbm,
+        scratch_shapes=[
+            V((rows, D), bf), V((2 * hg, own), f32),
+            V((Z, hu, fsub), f32), V((hu, fsub), f32), V((Z, hd, dsub), f32), V((hd, dsub), f32),
+            V((Z * 2 * hg, own), bf), V((Z, hu, fsub), bf), V((Z * 2 * hu, fsub), bf),
+            V((Z, hd, dsub), bf), V((Z, 2 * hd, dsub), bf),
+            V((Z, T, rows, own), bf), V((rows, D), bf), V((Z, T, rows, own), bf),
+            V((Z, 2, rows, own), bf), V(block, bf), V(block, bf), V(block, bf), V(block, bf),
+            V((T, rows, own), bf),
+            dma((4 + 2 * Z,)), dma((3, Z)), dma((3, Z)), dma((3, Z)), dma((3, Z)),
+            dma((Z,)), dma((Z,)), dma((Z,)), dma((Z,)), dma((Z, 2)), dma((Z, 2)),
+            dma((Z, 2)), dma((Z, 2)), dma((Z,)), dma((Z,)), dma((Z,)), dma((Z,)),
+            dma((3,)), dma((3,)), dma((4,)),
+        ],
+        compiler_params=pltpu.CompilerParams(
+            collective_id=0, has_side_effects=True, vmem_limit_bytes=60 * 1024 * 1024
+        ),
+    )(
+        tokens, mix_gain[None], group_weight, group_scale, mlp_gain[None],
+        up_weight, up_scale, down_weight, down_scale,
+    )
+
+
+def fits(mesh):
+    shape = mesh.shape
+    return shape["rep"] == 2 and shape["tp"] == GROUPS and shape["fs"] == shape["tp"]
+
+
 def solution(mesh):
     in_specs = (
         P(("rep", "fs"), None),
@@ -95,4 +382,5 @@
         P(),
     )
     out_specs = P(("rep", "fs"), None)
-    return jax.shard_map(body, mesh=mesh, in_specs=in_specs, out_specs=out_specs, check_vma=False)
+    chosen = functools.partial(fused, mesh.shape) if fits(mesh) else body
+    return jax.shard_map(chosen, mesh=mesh, in_specs=in_specs, out_specs=out_specs, check_vma=False)

time: 405 us -> 139 us (0.34)
  waiting for transfers between devices: 346 us -> 0 us
  Pallas kernels: 0 us -> 137 us
  blocking collectives: 15.3 us -> 0 us
  other arithmetic: 14.9 us -> 0 us
  matrix products: 13.9 us -> 0 us
  between operations: 13.2 us -> 0.01 us
    all_gather x3 -> x0, waiting for transfers between devices: 311 us -> none  [the longest x1 149 us: body(): lax.all_gather(up_weight.astype(jnp.bfloat16), 'fs', axis=0, tiled=True)]
    pallas_call x0 -> x1, Pallas kernels: none -> 137 us  [fused(): pl.pallas_call(functools.partial(ring_kernel, sizes), out_shape=jax.Shape...]
    psum x1 -> x0, waiting for transfers between devices: 34.1 us -> none  [body(): lax.psum(partial_value.astype(jnp.bfloat16), 'tp').astype(jnp.float32)]
    all_gather x1 -> x0, blocking collectives: 15.3 us -> none  [body(): lax.all_gather(group_weight.astype(jnp.bfloat16), 'fs', axis=0, tiled=True)]
    dot_general x3 -> x0, matrix products: 13.9 us -> none  [the longest x1 11.7 us: body(): jnp.dot(hidden, lax.all_gather(down_weight.astype(jnp.bfloat16), 'fs', ax...]
    convert_element_type x7 -> x0, other arithmetic: 11.8 us -> none  [the longest x1 3.85 us: body(): up_weight.astype(jnp.bfloat16)]
  transfers between devices with their start and end apart: 4 -> 0, of which waited for: 4 -> 0; matrix products, arithmetic and copies ran while one was open for 2% -> 0% of each run, Pallas kernels for 0% -> 0%
where the time goes in v1:
time: 139 us
  Pallas kernels  137 us (99%)
  local copies, waits for them, and re-layouts  2.3 us (2%)
    pallas_call x1, Pallas kernels, fused(): pl.pallas_call(functools.partial(ring_kernel, sizes), out_shape=jax.Shape...  137 us

profile of v1, /device:TPU:1, one launch (start us, length us, event | category | flops | bytes accessed | tf_op | source)
XLA Modules:
  0.0 139.0 jit_solution(10255176289974071999)
XLA Ops:
  0.0 136.7 %shard_map.91 = bf16[256,2048]{1,0:T(8,128)(2,1)} custom-call(bf16[256,2048]{1,0:T(8,128)(2,1)} %tok_h.1, f32[1,2048]{1,0:T(1,128)} %bitcast.2, f32[128,512]{1,0:T(8,128)} %gw_h.1, f32[1,512]{1,0:T(1,128)} %gs.1, f32[1,2048]{1,0:T(1,128)} %bitcast.3, f32[512,2048]{1,0:T(8,128)} %up_h.1, f32[1,2048]{1,0:T(1,128)} %us.1, f32[2048,512]{1,0:T(8,128)} %dn_h.1, ...), custom_call_target="tpu_custom_call" | custom-call | tf_op jit(solution)/shard_map/pallas_call | solution.py:340
  136.7 2.3 %copy.11 = bf16[256,2048]{1,0:T(8,128)(2,1)} copy(bf16[256,2048]{1,0:T(8,128)(2,1)} %shard_map.91) | data formatting | bytes 2097152

commit v2 on v1

--- a/solution.py
+++ b/solution.py
@@ -123,9 +123,11 @@
     load("gw", gw_h, gwf, 0)
     load("tok", tok_h, tok, 1)
     order = list(range(1, Z)) + [0]
-    for i, d in enumerate(order):
+    for d in order:
         zd = zat(d)
         load(("up", d), up_h.at[pl.ds(mul(r, hu), hu), pl.ds(mul(zd, fsub), fsub)], upf.at[d], 2 + d)
+    for d in order:
+        zd = zat(d)
         load(("dn", d), dn_h.at[pl.ds(pl.multiple_of(zd * 2 * hd + r * hd, hd), hd), :], dnf.at[d], 2 + Z + d)
     load("upo", up_h.at[pl.ds(mul(peer_r, hu), hu), pl.ds(mul(z, fsub), fsub)], upo, 2 + 2 * Z)
     load("dno", dn_h.at[pl.ds(pl.multiple_of(z * 2 * hd + peer_r * hd, hd), hd), :], dno, 3 + 2 * Z)
@@ -134,6 +136,8 @@
     peers = [(r, zat(d), t) for d in range(1, Z)] + [(peer_r, z, t), (r, z, xp), (r, z, cp)]
     for p in peers:
         pl.semaphore_signal(barrier, inc=1, device_id=p, device_id_type=MESH)
+    loads["gw"].wait()
+    gwg[pl.ds(mul(z, 2 * hg), 2 * hg), :] = gwf[...].astype(bf)
     pl.semaphore_wait(barrier, len(peers))
 
     sends = []
@@ -143,10 +147,19 @@
             src_ref=src, dst_ref=dst, send_sem=ss, recv_sem=rs, device_id=dev, device_id_type=MESH
         )
 
-    def send(src, dst, ss, rs, dev):
-        c = remote(src, dst, ss, rs, dev)
-        c.start()
-        sends.append(c)
+    def send(src, dst, ss, rs, dev, when=None):
+        if when is None:
+            remote(src, dst, ss, rs, dev).start()
+        else:
+            pl.when(when)(lambda: remote(src, dst, ss, rs, dev).start())
+        sends.append((when, (src, dst, ss, rs, dev)))
+
+    def drain():
+        for when, args in sends:
+            if when is None:
+                remote(*args).wait_send()
+            else:
+                pl.when(when)(lambda args=args: remote(*args).wait_send())
 
     def got(dst, ss, rs):
         remote(dst, dst, ss, rs, (peer_r, z, t)).wait_recv()
@@ -162,20 +175,17 @@
 
     place = (gw_at, up_at, dn_at)
 
-    loads["gw"].wait()
-    gwg[pl.ds(mul(z, 2 * hg), 2 * hg), :] = gwf[...].astype(bf)
-    for i, d in enumerate(range(1, Z)):
-        loads[("up", d)].wait()
-        ups[d] = upf[d].astype(bf)
-        if i == 0:
-            for e in range(1, Z):
-                send(gw_at(z, r), gw_at(z, r), sw.at[0, e], rw.at[0, z], (r, zat(e), t))
-        loads[("dn", d)].wait()
-        dns[d] = dnf[d].astype(bf)
     for d in range(1, Z):
-        send(ups.at[d], up_at(z, r), sw.at[1, d], rw.at[1, z], (r, zat(d), t))
-    for d in range(1, Z):
-        send(dns.at[d], dn_at(z, r), sw.at[2, d], rw.at[2, z], (r, zat(d), t))
+        send(gw_at(z, r), gw_at(z, r), sw.at[0, d], rw.at[0, z], (r, zat(d), t))
+    ready = []
+    for w, key, raw, cast in ((1, "up", upf, ups), (2, "dn", dnf, dns)):
+        for d in range(1, Z):
+            loads[(key, d)].wait()
+            cast[d] = raw[d].astype(bf)
+            ready.append((cast.at[d], place[w](z, r), sw.at[w, d], rw.at[w, z], (r, zat(d), t)))
+            if len(ready) > 1:
+                send(*ready.pop(0))
+    send(*ready.pop(0))
     loads[("up", 0)].wait()
     upg[pl.ds(pl.multiple_of(z * 2 * hu + r * hu, hu), hu), :] = upf[0].astype(bf)
     loads["upo"].wait()
@@ -219,105 +229,143 @@
     swapped(0)
     mixed = jnp.dot(pooled, gwg[...], preferred_element_type=f32) * gs[...]
     car[z, t] = (mine + mixed).astype(bf)
-    blk = car.at[z, t]
-    send(blk, blk, scx.at[0], rcx.at[z], (r, z, xp))
-    send(blk, blk, scc.at[0, 0], rcc.at[z, 0], (r, z, cp))
-    for d in range(1, Z):
-        send(blk, blk, scz.at[d], rcz.at[z], (r, zat(d), t))
-
-    def from_x(d):
-        src = zat(Z - d)
-        got(car.at[src, xp], scx.at[d], rcx.at[src])
-        b = car.at[src, xp]
-        send(b, b, scc.at[d, 1], rcc.at[src, 1], (r, z, cp))
+    H = rows // LENGTH
+    hr = LENGTH
+    side = 1 - 2 * lax.div(z, Z // 2)
+
+    inner = lax.div(Z - 1 - side * (Z - 1 - 2 * z), 2)
+
+    def src_of(d):
+        if d == 0:
+            return z
+        near = (d + 1) // 2 if d % 2 else -(d // 2)
+        both_sides = lax.div(2 * inner - d + 2 * Z, 2 * Z)
+        return z + side * (both_sides * near + (1 - both_sides) * (d - inner))
+
+    def half(h):
+        return pl.ds(h * hr, hr)
+
+    def to_x(src, h):
+        b = car.at[src, t, half(h)]
+        send(b, b, scx.at[src, h], rcx.at[src, h], (r, z, xp))
+
+    def to_core(src, h, q, k):
+        b = car.at[src, q, half(h)]
+        send(b, b, scc.at[src, k, h], rcc.at[src, k, h], (r, z, cp))
+
+    def to_z(src, h, when_up, when_down):
+        b = car.at[src, t, half(h)]
+        send(b, b, scz.at[0, src, h], rcz.at[src, h], (r, lax.rem(z + 1, Z), t), when_up)
+        send(b, b, scz.at[1, src, h], rcz.at[src, h], (r, lax.rem(z + Z - 1, Z), t), when_down)
+
+    for h in range(H):
+        to_z(z, h, z < Z - 1, z > 0)
+        to_x(z, h)
+        to_core(z, h, t, 0)
+
+    def arrive(d, h):
+        src = src_of(d)
+        got(car.at[src, t, half(h)], scz.at[0, src, h], rcz.at[src, h])
+        to_z(src, h, (src < z) & (z < Z - 1), (src > z) & (z > 0))
+        to_x(src, h)
+        to_core(src, h, t, 0)
+
+    def from_x(d, h):
+        src = src_of(d)
+        got(car.at[src, xp, half(h)], scx.at[src, h], rcx.at[src, h])
+        to_core(src, h, xp, 1)
 
     swap(1)
-    from_x(0)
+    for h in range(H):
+        from_x(0, h)
     swap(2)
-    for d in range(1, Z):
-        src = zat(Z - d)
-        b = car.at[src, t]
-        got(b, scz.at[d], rcz.at[src])
-        send(b, b, scx.at[d], rcx.at[src], (r, z, xp))
-        send(b, b, scc.at[d, 0], rcc.at[src, 0], (r, z, cp))
     swapped(1)
     swapped(2)
 
-    def compute(d):
-        src = zat(Z - d)
-        if d > 0:
-            from_x(d)
-        got(car.at[src, cp], scc.at[d, 0], rcc.at[src, 0])
-        got(car.at[src, cxp], scc.at[d, 1], rcc.at[src, 1])
-        total = jnp.zeros((rows, 1), f32)
+    def compute(d, h):
+        src = src_of(d)
+        hs = half(h)
+        got(car.at[src, cp, hs], scc.at[src, 0, h], rcc.at[src, 0, h])
+        got(car.at[src, cxp, hs], scc.at[src, 1, h], rcc.at[src, 1, h])
+        total = jnp.zeros((hr, 1), f32)
         for q in range(T):
-            c = car[src, q].astype(f32)
+            c = car[src, q, hs].astype(f32)
             total += jnp.sum(c * c, axis=-1, keepdims=True)
         scale = lax.rsqrt(total / D + norm_eps)
         for q in range(T):
             part = slice(q * own, (q + 1) * own)
-            xn[:, part] = (car[src, q].astype(f32) * scale * lg[:, part]).astype(bf)
+            xn[:, part] = (car[src, q, hs].astype(f32) * scale * lg[:, part]).astype(bf)
         pre = jnp.dot(xn[...], upg[...], preferred_element_type=f32)
         pre = jnp.maximum(pre * us[:, pl.ds(mul(z, fsub), fsub)], 0.0)
         hidden = (pre * pre).astype(bf)
         for q in range(T):
             part = slice(q * own, (q + 1) * own)
             p = jnp.dot(hidden, dng[q], preferred_element_type=f32) * ds[:, part]
-            pb[src, q] = p.astype(bf)
-        send(pb.at[src, cxp], ra.at[src, 1], sa.at[d, 1], ra_s.at[src, 1], (r, z, cp))
-        send(pb.at[src, cp], ra.at[src, 0], sa.at[d, 0], ra_s.at[src, 0], (r, z, cp))
-
-    def over_x(d):
-        src = zat(Z - d)
-        got(ra.at[src, 1], sa.at[d, 1], ra_s.at[src, 1])
-        sx[src] = (pb[src, xp].astype(f32) + ra[src, 1].astype(f32)).astype(bf)
-        send(sx.at[src], rb.at[src], sb.at[d], rb_s.at[src], (r, z, xp))
-
-    def over_z(d):
-        src = zat(Z - d)
-        got(ra.at[src, 0], sa.at[d, 0], ra_s.at[src, 0])
-        got(rb.at[src], sb.at[d], rb_s.at[src])
-        both = pb[src, t].astype(f32) + ra[src, 0].astype(f32) + rb[src].astype(f32)
+            pb[src, q, hs] = p.astype(bf)
+        for k, q in ((1, cxp), (0, cp)):
+            send(pb.at[src, q, hs], ra.at[src, k, hs], sa.at[src, k, h], ra_s.at[src, k, h], (r, z, cp))
+
+    def over_x(d, h):
+        src = src_of(d)
+        hs = half(h)
+        got(ra.at[src, 1, hs], sa.at[src, 1, h], ra_s.at[src, 1, h])
+        sx[src, hs] = (pb[src, xp, hs].astype(f32) + ra[src, 1, hs].astype(f32)).astype(bf)
+        send(sx.at[src, hs], rb.at[src, hs], sb.at[src, h], rb_s.at[src, h], (r, z, xp))
+
+    def over_z(d, h):
+        src = src_of(d)
+        hs = half(h)
+        got(ra.at[src, 0, hs], sa.at[src, 0, h], ra_s.at[src, 0, h])
+        got(rb.at[src, hs], sb.at[src, h], rb_s.at[src, h])
+        both = pb[src, t, hs].astype(f32) + ra[src, 0, hs].astype(f32) + rb[src, hs].astype(f32)
         if d == 0:
             return both
-        sz[src] = both.astype(bf)
-        send(sz.at[src], rc.at[z], st.at[d], rt.at[z], (r, src, t))
-
-    kept = None
-    for i in range(Z + 2):
-        if i < Z:
-            compute(i)
-        if 0 <= i - 1 < Z:
-            over_x(i - 1)
-        if 0 <= i - 2 < Z:
-            if i - 2 > 0:
-                over_z(i - 2)
-    acc = over_z(0)
-    acc += car[z, t].astype(f32)
-    for d in range(1, Z):
-        src = zat(d)
-        got(rc.at[src], st.at[d], rt.at[src])
-        acc += rc[src].astype(f32)
-    og[t] = acc.astype(bf)
-    send(og.at[t], og.at[t], so.at[0], ro.at[0], (r, z, xp))
-    send(og.at[t], og.at[t], so.at[1], ro.at[1], (r, z, cp))
+        sz[src, hs] = both.astype(bf)
+        send(sz.at[src, hs], rc.at[z, hs], st.at[src, h], rt.at[z, h], (r, src, t))
+
+    units = [(d, h) for d in range(Z) for h in range(H)]
+    lead = 4
+    for i in range(len(units) + lead):
+        for lag, stage in enumerate((arrive, from_x, compute, over_x, over_z)):
+            if 0 <= i - lag < len(units):
+                d, h = units[i - lag]
+                if d > 0 or stage in (compute, over_x):
+                    stage(d, h)
+
     writes = []
 
-    def write(q, k):
-        c = pltpu.make_async_copy(og.at[q], out_h.at[:, pl.ds(mul(q, own), own)], wr.at[k])
+    def write(q, k, h):
+        c = pltpu.make_async_copy(
+            og.at[q, half(h)], out_h.at[half(h), pl.ds(mul(q, own), own)], wr.at[k, h]
+        )
         c.start()
         writes.append(c)
 
-    write(t, 0)
-    got(og.at[xp], so.at[0], ro.at[0])
-    send(og.at[xp], og.at[xp], so.at[2], ro.at[2], (r, z, cp))
-    write(xp, 1)
-    got(og.at[cp], so.at[1], ro.at[1])
-    write(cp, 2)
-    got(og.at[cxp], so.at[2], ro.at[2])
-    write(cxp, 3)
-    for c in sends:
-        c.wait_send()
+    def pass_on(q, k, dev, h):
+        b = og.at[q, half(h)]
+        send(b, b, so.at[k, h], ro.at[k, h], dev)
+
+    for h in range(H):
+        hs = half(h)
+        acc = over_z(0, h) + car[z, t, hs].astype(f32)
+        for d in range(1, Z):
+            src = src_of(d)
+            got(rc.at[src, hs], st.at[src, h], rt.at[src, h])
+            acc += rc[src, hs].astype(f32)
+        og[t, hs] = acc.astype(bf)
+        pass_on(t, 0, (r, z, xp), h)
+        pass_on(t, 1, (r, z, cp), h)
+        write(t, 0, h)
+    for h in range(H):
+        got(og.at[xp, half(h)], so.at[0, h], ro.at[0, h])
+        pass_on(xp, 2, (r, z, cp), h)
+        write(xp, 1, h)
+    for h in range(H):
+        got(og.at[cp, half(h)], so.at[1, h], ro.at[1, h])
+        write(cp, 2, h)
+        got(og.at[cxp, half(h)], so.at[2, h], ro.at[2, h])
+        write(cxp, 3, h)
+    drain()
     for c in writes:
         c.wait()
 
@@ -337,6 +385,7 @@
     sizes = (Z, T, rows, D, own, hg, hu, hd, fsub, dsub)
     V = pltpu.VMEM
     block = (Z, rows, own)
+    H = rows // LENGTH
     return pl.pallas_call(
         functools.partial(ring_kernel, sizes),
         out_shape=jax.ShapeDtypeStruct((rows, D), bf),
@@ -347,13 +396,13 @@
             V((Z, hu, fsub), f32), V((hu, fsub), f32), V((Z, hd, dsub), f32), V((hd, dsub), f32),
             V((Z * 2 * hg, own), bf), V((Z, hu, fsub), bf), V((Z * 2 * hu, fsub), bf),
             V((Z, hd, dsub), bf), V((Z, 2 * hd, dsub), bf),
-            V((Z, T, rows, own), bf), V((rows, D), bf), V((Z, T, rows, own), bf),
+            V((Z, T, rows, own), bf), V((LENGTH, D), bf), V((Z, T, rows, own), bf),
             V((Z, 2, rows, own), bf), V(block, bf), V(block, bf), V(block, bf), V(block, bf),
             V((T, rows, own), bf),
             dma((4 + 2 * Z,)), dma((3, Z)), dma((3, Z)), dma((3, Z)), dma((3, Z)),
-            dma((Z,)), dma((Z,)), dma((Z,)), dma((Z,)), dma((Z, 2)), dma((Z, 2)),
-            dma((Z, 2)), dma((Z, 2)), dma((Z,)), dma((Z,)), dma((Z,)), dma((Z,)),
-            dma((3,)), dma((3,)), dma((4,)),
+            dma((2, Z, H)), dma((Z, H)), dma((Z, H)), dma((Z, H)), dma((Z, 2, H)), dma((Z, 2, H)),
+            dma((Z, 2, H)), dma((Z, 2, H)), dma((Z, H)), dma((Z, H)), dma((Z, H)), dma((Z, H)),
+            dma((3, H)), dma((3, H)), dma((4, H)),
         ],
         compiler_params=pltpu.CompilerParams(
             collective_id=0, has_side_effects=True, vmem_limit_bytes=60 * 1024 * 1024

time: 139 us -> 132 us (0.950)
  Pallas kernels: 137 us -> 130 us
    pallas_call x1, Pallas kernels: 137 us -> 130 us  [fused(): pl.pallas_call(functools.partial(ring_kernel, sizes), out_shape=jax.Shape...]
where the time goes in v2:
time: 132 us
  Pallas kernels  130 us (98%)
  local copies, waits for them, and re-layouts  2.3 us (2%)
    pallas_call x1, Pallas kernels, fused(): pl.pallas_call(functools.partial(ring_kernel, sizes), out_shape=jax.Shape...  130 us

profile of v2, /device:TPU:1, one launch (start us, length us, event | category | flops | bytes accessed | tf_op | source)
XLA Modules:
  0.0 131.9 jit_solution(121904306699632003)
XLA Ops:
  0.0 129.6 %shard_map.91 = bf16[256,2048]{1,0:T(8,128)(2,1)} custom-call(bf16[256,2048]{1,0:T(8,128)(2,1)} %tok_h.1, f32[1,2048]{1,0:T(1,128)} %bitcast.2, f32[128,512]{1,0:T(8,128)} %gw_h.1, f32[1,512]{1,0:T(1,128)} %gs.1, f32[1,2048]{1,0:T(1,128)} %bitcast.3, f32[512,2048]{1,0:T(8,128)} %up_h.1, f32[1,2048]{1,0:T(1,128)} %us.1, f32[2048,512]{1,0:T(8,128)} %dn_h.1, ...), custom_call_target="tpu_custom_call" | custom-call | tf_op jit(solution)/shard_map/pallas_call | solution.py:389
  129.6 2.3 %copy.11 = bf16[256,2048]{1,0:T(8,128)(2,1)} copy(bf16[256,2048]{1,0:T(8,128)(2,1)} %shard_map.91) | data formatting | bytes 2097152

commit v3 on v2

--- a/solution.py
+++ b/solution.py
@@ -95,7 +95,7 @@
     out_h,
     tok, gwf, upf, upo, dnf, dno,
     gwg, ups, upg, dns, dng,
-    car, xn, pb, ra, sx, rb, sz, rc, og,
+    car, xn, hid, pb, ra, sx, rb, sz, rc, og,
     ld, sw, rw, sy, ry, scz, rcz, scx, rcx, scc, rcc,
     sa, ra_s, sb, rb_s, st, rt, so, ro, wr,
 ):
@@ -183,9 +183,8 @@
             loads[(key, d)].wait()
             cast[d] = raw[d].astype(bf)
             ready.append((cast.at[d], place[w](z, r), sw.at[w, d], rw.at[w, z], (r, zat(d), t)))
-            if len(ready) > 1:
+            if w == 1 and d > 1 or w == 2 and d == 1:
                 send(*ready.pop(0))
-    send(*ready.pop(0))
     loads[("up", 0)].wait()
     upg[pl.ds(pl.multiple_of(z * 2 * hu + r * hu, hu), hu), :] = upf[0].astype(bf)
     loads["upo"].wait()
@@ -214,11 +213,14 @@
         pooled.append((summed / divisor - part.astype(f32)).astype(bf))
     pooled = jnp.concatenate(pooled, axis=0)
 
+    def swap_one(w, d):
+        src = zat(Z - d)
+        got(place[w](src, r), sw.at[w, d], rw.at[w, src])
+        send(place[w](src, r), place[w](src, r), sy.at[w, d], ry.at[w, src], (peer_r, z, t))
+
     def swap(w):
         for d in range(1, Z):
-            src = zat(Z - d)
-            got(place[w](src, r), sw.at[w, d], rw.at[w, src])
-            send(place[w](src, r), place[w](src, r), sy.at[w, d], ry.at[w, src], (peer_r, z, t))
+            swap_one(w, d)
 
     def swapped(w):
         for d in range(1, Z):
@@ -262,6 +264,8 @@
         to_z(z, h, z < Z - 1, z > 0)
         to_x(z, h)
         to_core(z, h, t, 0)
+    for args in ready:
+        send(*args)
 
     def arrive(d, h):
         src = src_of(d)
@@ -278,11 +282,17 @@
     swap(1)
     for h in range(H):
         from_x(0, h)
-    swap(2)
+    for d in range(1, Z):
+        for h in range(H):
+            arrive(d, h)
+            if d > 1:
+                from_x(d - 1, h)
+        swap_one(2, d)
+    for h in range(H):
+        from_x(Z - 1, h)
     swapped(1)
-    swapped(2)
-
-    def compute(d, h):
+
+    def up(d, h):
         src = src_of(d)
         hs = half(h)
         got(car.at[src, cp, hs], scc.at[src, 0, h], rcc.at[src, 0, h])
@@ -297,7 +307,12 @@
             xn[:, part] = (car[src, q, hs].astype(f32) * scale * lg[:, part]).astype(bf)
         pre = jnp.dot(xn[...], upg[...], preferred_element_type=f32)
         pre = jnp.maximum(pre * us[:, pl.ds(mul(z, fsub), fsub)], 0.0)
-        hidden = (pre * pre).astype(bf)
+        hid[src, hs] = (pre * pre).astype(bf)
+
+    def down(d, h):
+        src = src_of(d)
+        hs = half(h)
+        hidden = hid[src, hs]
         for q in range(T):
             part = slice(q * own, (q + 1) * own)
             p = jnp.dot(hidden, dng[q], preferred_element_type=f32) * ds[:, part]
@@ -323,13 +338,17 @@
         sz[src, hs] = both.astype(bf)
         send(sz.at[src, hs], rc.at[z, hs], st.at[src, h], rt.at[z, h], (r, src, t))
 
-    units = [(d, h) for d in range(Z) for h in range(H)]
-    lead = 4
-    for i in range(len(units) + lead):
-        for lag, stage in enumerate((arrive, from_x, compute, over_x, over_z)):
+    for d in range(Z):
+        for h in range(H):
+            up(d, h)
+    swapped(2)
+    units = [(d, h) for d in range(Z - 1, -1, -1) for h in range(H)]
+    stages = (down, over_x, over_z)
+    for i in range(len(units) + len(stages) - 1):
+        for lag, stage in enumerate(stages):
             if 0 <= i - lag < len(units):
                 d, h = units[i - lag]
-                if d > 0 or stage in (compute, over_x):
+                if d > 0 or stage is not over_z:
                     stage(d, h)
 
     writes = []
@@ -396,7 +415,7 @@
             V((Z, hu, fsub), f32), V((hu, fsub), f32), V((Z, hd, dsub), f32), V((hd, dsub), f32),
             V((Z * 2 * hg, own), bf), V((Z, hu, fsub), bf), V((Z * 2 * hu, fsub), bf),
             V((Z, hd, dsub), bf), V((Z, 2 * hd, dsub), bf),
-            V((Z, T, rows, own), bf), V((LENGTH, D), bf), V((Z, T, rows, own), bf),
+            V((Z, T, rows, own), bf), V((LENGTH, D), bf), V((Z, rows, fsub), bf), V((Z, T, rows, own), bf),
             V((Z, 2, rows, own), bf), V(block, bf), V(block, bf), V(block, bf), V(block, bf),
             V((T, rows, own), bf),
             dma((4 + 2 * Z,)), dma((3, Z)), dma((3, Z)), dma((3, Z)), dma((3, Z)),

time: 132 us -> 121 us (0.917)
  Pallas kernels: 130 us -> 118 us
    pallas_call x1, Pallas kernels: 130 us -> 118 us  [fused(): pl.pallas_call(functools.partial(ring_kernel, sizes), out_shape=jax.Shape...]
where the time goes in v3:
time: 121 us; the launch traced here: 120 us
  Pallas kernels  118 us (98%)
  local copies, waits for them, and re-layouts  2.3 us (2%)
    pallas_call x1, Pallas kernels, fused(): pl.pallas_call(functools.partial(ring_kernel, sizes), out_shape=jax.Shape...  118 us

profile of v3, /device:TPU:1, one launch (start us, length us, event | category | flops | bytes accessed | tf_op | source)
XLA Modules:
  0.0 120.5 jit_solution(1050311871532785350)
XLA Ops:
  0.0 118.2 %shard_map.91 = bf16[256,2048]{1,0:T(8,128)(2,1)} custom-call(bf16[256,2048]{1,0:T(8,128)(2,1)} %tok_h.1, f32[1,2048]{1,0:T(1,128)} %bitcast.2, f32[128,512]{1,0:T(8,128)} %gw_h.1, f32[1,512]{1,0:T(1,128)} %gs.1, f32[1,2048]{1,0:T(1,128)} %bitcast.3, f32[512,2048]{1,0:T(8,128)} %up_h.1, f32[1,2048]{1,0:T(1,128)} %us.1, f32[2048,512]{1,0:T(8,128)} %dn_h.1, ...), custom_call_target="tpu_custom_call" | custom-call | tf_op jit(solution)/shard_map/pallas_call | solution.py:408
  118.2 2.3 %copy.11 = bf16[256,2048]{1,0:T(8,128)(2,1)} copy(bf16[256,2048]{1,0:T(8,128)(2,1)} %shard_map.91) | data formatting | bytes 2097152
